TPU v7x, 128 devices: a whole 4x4x4 slice. The times are simulated.
128 devices in a mesh: sp: 32 (over z, y, core), tp: 4 (over x).
Axes of the slice: x: 4, y: 4, z: 4, core: 2. Of those that a mesh axis runs over, the one named last changes fastest.
Arguments:
- conv_input: bfloat16 [16384, 1024], P('sp', 'tp'), may hold values from -6 to 6
- gate_inner: bfloat16 [16384, 1024], P('sp', 'tp'), may hold values from -6 to 6
- gate_outer: bfloat16 [16384, 1024], P('sp', 'tp'), may hold values from -6 to 6
- conv_taps: bfloat16 [3, 1024], P(None, 'tp'), may hold values from -3.5 to 3.5
- doc_ids: int32 [16384], P('sp'), may hold values from 0 to 15, never falling along the last dimension, each value on 1 to 2048 neighbouring positions
- residual_in: bfloat16 [16384, 2048], P(('sp', 'tp')), may hold values from -6 to 6
- out_proj: bfloat16 [1024, 2048], replicated, may hold values from -0.1875 to 0.1875
- norm_gain: float32 [2048], replicated, may hold values from 0.1 to 1.9
- expert_ids: int32 [16384, 2], P(('sp', 'tp')), may hold values from 0 to 127, all different within a row; in each aligned block of 128 rows (0 to 127, 128 to 255, ...) at most 4 rows name the same one
- expert_weights: float32 [16384, 2], P(('sp', 'tp')), may hold values from 0.2 to 1
- gate_proj: bfloat16 [128, 2048, 1024], P(('sp', 'tp')), may hold values from -0.125 to 0.125
- up_proj: bfloat16 [128, 2048, 1024], P(('sp', 'tp')), may hold values from -0.125 to 0.125
- down_proj: bfloat16 [128, 1024, 2048], P(('sp', 'tp')), may hold values from -0.1875 to 0.1875
Outputs:
- layer_out: bfloat16 [16384, 2048], P(('sp', 'tp'))
Inputs may be any that keep to these rules, and one draw needn't show every extreme that they name: `doc_ids`: never falls along positions; each document has at most 2048 positions. `expert_ids`: each row names 2 different experts; within the rows of one device, aligned blocks of 128 rows, no expert is named more than 4 times, a bound that some block reaches.
All inputs are finite; a program needn't handle non-finite values.
Results may differ from a plain program's by a relative error of at most 0.009.
Values may be sent and summed in bfloat16 or wider, within the bound.
No kernel may reach another device: no remote copies, remote signals or barrier semaphores. Data moves between devices by JAX's collectives and lax.ppermute only.
A program may use at most 64 MiB of HBM per device.

v0:
```python
import jax
import jax.numpy as jnp
from jax import lax
from jax.sharding import PartitionSpec as P


def from_behind(block, axis, distance):
    devices = range(lax.axis_size(axis))
    route = [(i - distance, i) for i in devices if i - distance in devices]
    return lax.ppermute(block, axis, route)


def expert_rows(arrived, gate_weight, up_weight, down_weight):
    gate_value = jnp.dot(arrived, gate_weight, preferred_element_type=jnp.float32)
    up_value = jnp.dot(arrived, up_weight, preferred_element_type=jnp.float32)
    hidden = (jax.nn.silu(gate_value) * up_value).astype(jnp.bfloat16)
    return jnp.dot(hidden, down_weight, preferred_element_type=jnp.float32).astype(jnp.bfloat16)


def on_device(
    conv_input,
    gate_inner,
    gate_outer,
    conv_taps,
    doc_ids,
    residual_in,
    out_proj,
    norm_gain,
    expert_ids,
    expert_weights,
    gate_proj,
    up_proj,
    down_proj,
):
    inner_prod = conv_input.astype(jnp.float32) * gate_inner.astype(jnp.float32)
    earlier, earlier_docs = from_behind((inner_prod[-2:], doc_ids[-2:]), "sp", 1)
    padded = jnp.concatenate([earlier, inner_prod], axis=0)
    padded_docs = jnp.concatenate([earlier_docs, doc_ids], axis=0)
    length = inner_prod.shape[0]
    tap_values = conv_taps.astype(jnp.float32)
    one_back = jnp.where(
        (padded_docs[1 : length + 1] == doc_ids)[:, None], padded[1 : length + 1], 0.0
    )
    two_back = jnp.where((padded_docs[:length] == doc_ids)[:, None], padded[:length], 0.0)
    mixed_rows = tap_values[2] * inner_prod + tap_values[1] * one_back + tap_values[0] * two_back
    conv_out = (gate_outer.astype(jnp.float32) * mixed_rows).astype(jnp.bfloat16)
    row_count = residual_in.shape[0]
    regrouped = lax.all_to_all(conv_out, "tp", split_axis=0, concat_axis=1, tiled=True)
    mix = jnp.dot(regrouped, out_proj, preferred_element_type=jnp.float32).astype(jnp.bfloat16)
    carried = residual_in.astype(jnp.float32) + mix.astype(jnp.float32)
    normed = (
        carried * lax.rsqrt(jnp.mean(carried * carried, axis=1, keepdims=True) + 1e-06) * norm_gain
    ).astype(jnp.bfloat16)
    model_width = normed.shape[1]
    choose = expert_ids.shape[1]
    sp_count = lax.axis_size("sp")
    tp_count = lax.axis_size("tp")
    experts_total = sp_count * tp_count
    capacity = 2 * row_count * choose // experts_total
    flat_ids = expert_ids.reshape(-1)
    onehot = (flat_ids[:, None] == jnp.arange(experts_total, dtype=jnp.int32)[None, :]).astype(
        jnp.int32
    )
    slot_rank = jnp.sum((jnp.cumsum(onehot, axis=0) - 1) * onehot, axis=1)
    target = flat_ids * capacity + slot_rank
    sources = jnp.repeat(normed, choose, axis=0)
    outgoing = (
        jnp.zeros((experts_total * capacity, model_width), jnp.bfloat16).at[target].set(sources)
    )
    gate_weight = gate_proj[0]
    up_weight = up_proj[0]
    down_weight = down_proj[0]
    arrived = lax.all_to_all(
        outgoing.reshape(experts_total, capacity, model_width),
        ("sp", "tp"),
        split_axis=0,
        concat_axis=0,
        tiled=True,
    )
    item_count = arrived.shape[1]
    flat_rows = arrived.reshape(-1, model_width)
    result = expert_rows(flat_rows, gate_weight, up_weight, down_weight)
    result = result.reshape(experts_total, item_count, model_width)
    returned = lax.all_to_all(result, ("sp", "tp"), split_axis=0, concat_axis=0, tiled=True)
    picked = (
        returned.reshape(-1, model_width)[target]
        .reshape(row_count, choose, model_width)
        .astype(jnp.float32)
    )
    combined = carried + jnp.sum(expert_weights[:, :, None] * picked, axis=1)
    return combined.astype(jnp.bfloat16)


def solution(mesh):
    in_specs = (
        P("sp", "tp"),
        P("sp", "tp"),
        P("sp", "tp"),
        P(None, "tp"),
        P("sp"),
        P(("sp", "tp"), None),
        P(),
        P(),
        P(("sp", "tp"), None),
        P(("sp", "tp"), None),
        P(("sp", "tp"), None, None),
        P(("sp", "tp"), None, None),
        P(("sp", "tp"), None, None),
    )
    out_specs = P(("sp", "tp"), None)
    return jax.shard_map(
        on_device, mesh=mesh, in_specs=in_specs, out_specs=out_specs, check_vma=False
    )
```

profile of v0, /device:TPU:1, one launch (start us, length us, event | category | flops | bytes accessed | tf_op | source)
XLA Modules:
  0.0 143.9 jit_solution(9995977291659634800)
XLA Ops:
  0.0 1.2 convert_multiply_fusion
  1.2 4.6 %collective-permute-start.1 = (f32[2,256]{1,0:T(2,128)S(1)}, f32[2,256]{1,0:T(2,128)S(1)}, u32[]{:S(2)}, u32[]{:S(2)}) collective-permute-start(f32[2,256]{1,0:T(2,128)S(1)} %slice.48), channel_id=1, source_target_pairs={{0,4},{4,8},{8,12},{12,16},{16,20},{20,24},{24,28},{28,32},{32,36}... | collective-permute-start | bytes 6152 | tf_op jit(solution)/shard_map/ppermute | solution.py:10
  5.8 0.8 slice.35
  6.5 1.9 %collective-permute-start = (s32[2]{0:T(128)S(1)}, s32[2]{0:T(128)S(1)}, u32[]{:S(2)}, u32[]{:S(2)}) collective-permute-start(s32[2]{0:T(128)S(1)} %slice.35), channel_id=1, source_target_pairs={{0,4},{4,8},{8,12},{12,16},{16,20},{20,24},{24,28},{28,32},{32,36}... | collective-permute-start | bytes 32 | tf_op jit(solution)/shard_map/ppermute | solution.py:10
  8.4 0.8 copy.24
  9.2 0.1 eq.37
  9.4 0.1 eq.33
  9.5 0.7 broadcast_multiply_fusion
  10.2 0.8 fusion.31
  11.0 0.1 copy.26
  11.1 0.2 fusion.26
  11.4 0.1 add_add_fusion
  11.5 0.1 copy.23
  11.6 0.1 mul.103
  11.7 0.2 fusion.27
  11.9 0.0 collective-permute-done
  11.9 0.0 copy-done.4
  11.9 0.1 pad_add_fusion
  12.0 0.1 slice_compare_fusion.1
  12.1 0.0 collective-permute-done.1
  12.1 0.0 copy-done.2
  12.1 1.0 fusion.23
  13.1 4.0 %all-to-all-start = ((bf16[4,128,256]{2,1,0:T(8,128)(2,1)}), bf16[4,128,256]{2,1,0:T(8,128)(2,1)S(1)}, u32[]{:S(2)}, u32[]{:S(2)}) async-start(bf16[4,128,256]{2,1,0:T(8,128)(2,1)} %bitcast.3), calls=%async_computation | async-start | bytes 524288 | tf_op jit(solution)/shard_map/all_to_all | solution.py:48
  17.1 5.7 %all-to-all-done = bf16[4,128,256]{2,1,0:T(8,128)(2,1)S(1)} async-done(((bf16[4,128,256]{2,1,0:T(8,128)(2,1)}), bf16[4,128,256]{2,1,0:T(8,128)(2,1)S(1)}, u32[]{:S(2)}, u32[]{:S(2)}) %all-to-all-start) | async-done | bytes 262176 | tf_op jit(solution)/shard_map/all_to_all | solution.py:48
  22.8 0.2 copy.21
  23.0 0.0 copy-done.1
  23.0 0.0 copy-start.3
  23.0 3.0 %multiply_reduce_fusion.1 = (f32[128]{0:T(128)S(1)}, f32[128,2048]{1,0:T(8,128)S(1)}) fusion(bf16[128,1024]{0,1:T(8,128)(2,1)S(1)} %bitcast.35, bf16[1024,2048]{1,0:T(8,128)(2,1)} %param.19, bf16[128,2048]{1,0:T(8,128)(2,1)S(1)} %copy-done.1), kind=kOutput, calls=%fused_computation.16 | convolution fusion | flops 538443648 | bytes 6029824 | tf_op jit(solution)/shard_map/dot_general | solution.py:49
  26.0 0.0 copy-done.3
  26.0 0.2 multiply_convert_fusion.1
  26.2 0.6 broadcast_in_dim.36
  26.8 1.2 reshape.100
  28.1 3.5 %scatter_custom_fusion = bf16[512,2048]{1,0:T(8,128)(2,1)S(1)} fusion(s32[256]{0:T(256)S(1)} %bitcast.38, bf16[256,2048]{1,0:T(8,128)(2,1)} %reshape.100, bf16[]{:T(256)} %constant.6.clone.1), kind=kCustom, calls=%fused_computation.17 | custom fusion | bytes 2097664 | tf_op jit(solution)/shard_map/scatter | solution.py:68
  31.6 2.2 %reshape.83 = bf16[128,4,2048]{2,1,0:T(4,128)(2,1)} reshape(bf16[512,2048]{1,0:T(8,128)(2,1)S(1)} %scatter_custom_fusion) | data formatting | bytes 4194304 | tf_op jit(solution)/shard_map/reshape | solution.py:74
  33.8 40.5 %all_to_all.29 = bf16[128,4,2048]{2,1,0:T(4,128)(2,1)S(1)} all-to-all(bf16[128,4,2048]{2,1,0:T(4,128)(2,1)} %reshape.83), channel_id=1, replica_groups=mesh['sp'=32,'tp'=4] {'sp','tp'}, dimensions={0} | all-to-all | bytes 4194304 | tf_op jit(solution)/shard_map/all_to_all | solution.py:73
  74.3 2.0 %reshape.84 = bf16[512,2048]{1,0:T(8,128)(2,1)} reshape(bf16[128,4,2048]{2,1,0:T(4,128)(2,1)S(1)} %all_to_all.29) | data formatting | bytes 4194304 | tf_op jit(solution)/shard_map/reshape | solution.py:81
  76.4 6.6 %fusion.4 = f32[512,1024]{1,0:T(8,128)} fusion(bf16[512,2048]{1,0:T(8,128)(2,1)} %reshape.84, bf16[1,2048,1024]{2,1,0:T(8,128)(2,1)} %param.23), kind=kOutput, calls=%fused_computation.6 | convolution fusion | flops 2147483648 | bytes 8388608 | tf_op jit(solution)/shard_map/dot_general | solution.py:14
  83.0 0.0 copy-done
  83.0 9.9 %fusion.6 = bf16[512,2048]{1,0:T(8,128)(2,1)} fusion(bf16[1,1024,2048]{2,1,0:T(8,128)(2,1)} %param.25, f32[512,1024]{1,0:T(8,128)} %fusion.4, bf16[512,2048]{1,0:T(8,128)(2,1)S(1)} %copy-done, bf16[1,2048,1024]{2,1,0:T(8,128)(2,1)} %param.24), kind=kOutput, calls=%fused_computation.8 | convolution fusion | flops 4299161600 | bytes 14680064 | tf_op jit(solution)/shard_map/dot_general | solution.py:17
  92.9 4.1 %reshape.85 = bf16[128,4,2048]{2,1,0:T(4,128)(2,1)} reshape(bf16[512,2048]{1,0:T(8,128)(2,1)} %fusion.6) | data formatting | bytes 4194304 | tf_op jit(solution)/shard_map/reshape | solution.py:83
  97.0 5.0 %all-to-all-start.2 = ((bf16[128,4,2048]{2,1,0:T(4,128)(2,1)}), bf16[128,4,2048]{2,1,0:T(4,128)(2,1)}, u32[]{:S(2)}, u32[]{:S(2)}) async-start(bf16[128,4,2048]{2,1,0:T(4,128)(2,1)} %reshape.85), calls=%async_computation.2 | async-start | bytes 4194304 | tf_op jit(solution)/shard_map/all_to_all | solution.py:84
  102.0 0.1 copy.22
  102.1 30.4 %all-to-all-done.2 = bf16[128,4,2048]{2,1,0:T(4,128)(2,1)} async-done(((bf16[128,4,2048]{2,1,0:T(4,128)(2,1)}), bf16[128,4,2048]{2,1,0:T(4,128)(2,1)}, u32[]{:S(2)}, u32[]{:S(2)}) %all-to-all-start.2) | async-done | bytes 2097184 | tf_op jit(solution)/shard_map/all_to_all | solution.py:84
  132.6 2.5 %reshape.86 = bf16[512,2048]{1,0:T(8,128)(2,1)S(1)} reshape(bf16[128,4,2048]{2,1,0:T(4,128)(2,1)} %all-to-all-done.2) | data formatting | bytes 4194304 | tf_op jit(solution)/shard_map/reshape | solution.py:86
  135.1 2.3 %gather_fusion = bf16[256,2048]{1,0:T(8,128)(2,1)} fusion(bf16[512,2048]{1,0:T(8,128)(2,1)S(1)} %reshape.86, s32[1024]{0:T(1024)S(1)} %pad_clamp_fusion), kind=kCustom, calls=%fused_computation | custom fusion | bytes 2098176 | tf_op jit(solution)/shard_map/gather | solution.py:86
  137.4 2.4 %reshape.87 = f32[128,2,2048]{2,1,0:T(2,128)S(1)} reshape(bf16[256,2048]{1,0:T(8,128)(2,1)} %gather_fusion) | data formatting | bytes 3145728 | tf_op jit(solution)/shard_map/convert_element_type | solution.py:88
  139.8 3.2 %multiply_reduce_fusion = f32[128,2048]{1,0:T(8,128)S(1)} fusion(f32[128,2,2048]{2,1,0:T(2,128)S(1)} %reshape.87, f32[128,2]{1,0:T(8,128)S(1)} %copy.22), kind=kLoop, calls=%fused_computation.12 | loop fusion | flops 786432 | bytes 3146752 | tf_op jit(solution)/shard_map/reduce_sum | solution.py:90
  143.0 0.9 add_convert_fusion
  (14 shorter events, 0.1 us)
Async XLA Ops:
  0.0 11.9 %copy-start.4 = (s32[512]{0:T(512)S(1)}, s32[512]{0:T(512)}, u32[]{:S(2)}) copy-start(s32[512]{0:T(512)} %param.17) | copy-start | bytes 6148
  0.0 12.1 %copy-start.2 = (bf16[512,256]{1,0:T(8,128)(2,1)S(1)}, bf16[512,256]{1,0:T(8,128)(2,1)}, u32[]{:S(2)}) copy-start(bf16[512,256]{1,0:T(8,128)(2,1)} %param.15) | copy-start | bytes 786436
  0.0 23.0 %copy-start.1 = (bf16[128,2048]{1,0:T(8,128)(2,1)S(1)}, bf16[128,2048]{1,0:T(8,128)(2,1)}, u32[]{:S(2)}) copy-start(bf16[128,2048]{1,0:T(8,128)(2,1)} %param.18) | copy-start | bytes 1572868
  1.2 10.9 %collective-permute-start.1 = (f32[2,256]{1,0:T(2,128)S(1)}, f32[2,256]{1,0:T(2,128)S(1)}, u32[]{:S(2)}, u32[]{:S(2)}) collective-permute-start(f32[2,256]{1,0:T(2,128)S(1)} %slice.48), channel_id=1, source_target_pairs={{0,4},{4,8},{8,12},{12,16},{16,20},{20,24},{24,28},{28,32},{32,36}... | collective-permute-start | bytes 6152 | tf_op jit(solution)/shard_map/ppermute | solution.py:10
  6.5 5.4 %collective-permute-start = (s32[2]{0:T(128)S(1)}, s32[2]{0:T(128)S(1)}, u32[]{:S(2)}, u32[]{:S(2)}) collective-permute-start(s32[2]{0:T(128)S(1)} %slice.35), channel_id=1, source_target_pairs={{0,4},{4,8},{8,12},{12,16},{16,20},{20,24},{24,28},{28,32},{32,36}... | collective-permute-start | bytes 32 | tf_op jit(solution)/shard_map/ppermute | solution.py:10
  13.1 9.7 %all-to-all-start = ((bf16[4,128,256]{2,1,0:T(8,128)(2,1)}), bf16[4,128,256]{2,1,0:T(8,128)(2,1)S(1)}, u32[]{:S(2)}, u32[]{:S(2)}) async-start(bf16[4,128,256]{2,1,0:T(8,128)(2,1)} %bitcast.3), calls=%async_computation | async-start | bytes 524288 | tf_op jit(solution)/shard_map/all_to_all | solution.py:48
  23.0 3.0 %copy-start.3 = (f32[2048]{0:T(1024)S(1)}, f32[2048]{0:T(1024)}, u32[]{:S(2)}) copy-start(f32[2048]{0:T(1024)} %param.20) | copy-start | bytes 24580
  76.4 6.7 %copy-start = (bf16[512,2048]{1,0:T(8,128)(2,1)S(1)}, bf16[512,2048]{1,0:T(8,128)(2,1)}, u32[]{:S(2)}) copy-start(bf16[512,2048]{1,0:T(8,128)(2,1)} %reshape.84) | copy-start | bytes 6291460
  97.0 5.0 %copy-start.5 = (f32[128,2]{0,1:T(2,128)S(1)}, f32[128,2]{0,1:T(2,128)}, u32[]{:S(2)}) copy-start(f32[128,2]{0,1:T(2,128)} %param.22) | copy-start | bytes 3076
  97.0 35.5 %all-to-all-start.2 = ((bf16[128,4,2048]{2,1,0:T(4,128)(2,1)}), bf16[128,4,2048]{2,1,0:T(4,128)(2,1)}, u32[]{:S(2)}, u32[]{:S(2)}) async-start(bf16[128,4,2048]{2,1,0:T(4,128)(2,1)} %reshape.85), calls=%async_computation.2 | async-start | bytes 4194304 | tf_op jit(solution)/shard_map/all_to_all | solution.py:84
where the time goes:
time: 145 us; the launch traced here: 144 us
  blocking collectives  40.5 us (28%)
  waiting for transfers between devices  36.1 us (25%)
  local copies, waits for them, and re-layouts  24.3 us (17%)
  matrix products  19.6 us (14%)
  starting transfers between devices  15.5 us (11%)
  other arithmetic  7.76 us (5%)
    all_to_all x1, blocking collectives, on_device(): lax.all_to_all(outgoing.reshape(experts_total, capacity, model_width), ('...  40.5 us
    all_to_all x1, waiting for transfers between devices, on_device(): lax.all_to_all(result, ('sp', 'tp'), split_axis=0, concat_axis=0, tiled=T...  30.4 us
    dot_general x1, matrix products, expert_rows(): jnp.dot(hidden, down_weight, preferred_element_type=jnp.float32)  9.9 us
    dot_general x1, matrix products, expert_rows(): jnp.dot(arrived, gate_weight, preferred_element_type=jnp.float32)  6.65 us
    ppermute x2, starting transfers between devices, from_behind(): return lax.ppermute(block, axis, route)  6.49 us
    all_to_all x1, waiting for transfers between devices, on_device(): lax.all_to_all(conv_out, 'tp', split_axis=0, concat_axis=1, tiled=True)  5.69 us
    all_to_all x1, starting transfers between devices, on_device(): lax.all_to_all(result, ('sp', 'tp'), split_axis=0, concat_axis=0, tiled=T...  4.97 us
    reshape x1, local copies, waits for them, and re-layouts, on_device(): result = result.reshape(experts_total, item_count, model_width)  4.11 us
  transfers between devices with their start and end apart: 4, of which 2 were waited for; matrix products, arithmetic and copies ran while one was open for 3% of the time, Pallas kernels for 0%

commit v1 on v0

--- a/solution.py
+++ b/solution.py
@@ -2,6 +2,16 @@
 import jax.numpy as jnp
 from jax import lax
 from jax.sharding import PartitionSpec as P
+
+choose_regions = lambda array_dim, packet, device_axis, pos_dim: jnp.concatenate(
+    lax.all_to_all(
+        jnp.stack(jnp.split(packet, lax.axis_size(device_axis), axis=array_dim), axis=0),
+        axis_name=device_axis,
+        split_axis=0,
+        concat_axis=0,
+    ),
+    axis=pos_dim,
+)
 
 
 def from_behind(block, axis, distance):
@@ -45,7 +55,7 @@
     mixed_rows = tap_values[2] * inner_prod + tap_values[1] * one_back + tap_values[0] * two_back
     conv_out = (gate_outer.astype(jnp.float32) * mixed_rows).astype(jnp.bfloat16)
     row_count = residual_in.shape[0]
-    regrouped = lax.all_to_all(conv_out, "tp", split_axis=0, concat_axis=1, tiled=True)
+    regrouped = choose_regions(0, packet=conv_out, device_axis="tp", pos_dim=1)
     mix = jnp.dot(regrouped, out_proj, preferred_element_type=jnp.float32).astype(jnp.bfloat16)
     carried = residual_in.astype(jnp.float32) + mix.astype(jnp.float32)
     normed = (

time: 145 us -> 143 us (0.986)
  other arithmetic: 7.76 us -> 6.23 us
    unnamed x14 -> x21, local copies, waits for them, and re-layouts: 0.93 us -> 2.62 us
  transfers between devices with their start and end apart: 4 -> 4, of which waited for: 2 -> 2; matrix products, arithmetic and copies ran while one was open for 3% -> 1% of each run, Pallas kernels for 0% -> 0%
where the time goes in v1:
time: 143 us
  blocking collectives  40.5 us (28%)
  waiting for transfers between devices  36.1 us (25%)
  local copies, waits for them, and re-layouts  24.4 us (17%)
  matrix products  19.6 us (14%)
  starting transfers between devices  15.5 us (11%)
  other arithmetic  6.23 us (4%)
    all_to_all x1, blocking collectives, on_device(): lax.all_to_all(outgoing.reshape(experts_total, capacity, model_width), ('...  40.5 us
    all_to_all x1, waiting for transfers between devices, on_device(): lax.all_to_all(result, ('sp', 'tp'), split_axis=0, concat_axis=0, tiled=T...  30.4 us
    dot_general x1, matrix products, expert_rows(): jnp.dot(hidden, down_weight, preferred_element_type=jnp.float32)  9.9 us
    dot_general x1, matrix products, expert_rows(): jnp.dot(arrived, gate_weight, preferred_element_type=jnp.float32)  6.64 us
    ppermute x2, starting transfers between devices, from_behind(): return lax.ppermute(block, axis, route)  6.49 us
    all_to_all x1, waiting for transfers between devices, lax.all_to_all(jnp.stack(jnp.split(packet, lax.axis_size(device_axis), ax...  5.69 us
    all_to_all x1, starting transfers between devices, on_device(): lax.all_to_all(result, ('sp', 'tp'), split_axis=0, concat_axis=0, tiled=T...  4.98 us
    reshape x1, local copies, waits for them, and re-layouts, on_device(): result = result.reshape(experts_total, item_count, model_width)  4.09 us
  transfers between devices with their start and end apart: 4, of which 2 were waited for; matrix products, arithmetic and copies ran while one was open for 1% of the time, Pallas kernels for 0%

profile of v1, /device:TPU:1, one launch (start us, length us, event | category | flops | bytes accessed | tf_op | source)
XLA Modules:
  0.0 142.6 jit_solution(5676852584177588969)
XLA Ops:
  0.0 0.0 copy-start.2
  0.0 1.1 copy.16
  1.2 1.1 copy.17
  2.3 0.1 convert_multiply_fusion
  2.3 0.1 slice.48
  2.4 4.6 %collective-permute-start.1 = (f32[2,256]{0,1:T(8,128)S(1)}, f32[2,256]{0,1:T(8,128)S(1)}, u32[]{:S(2)}, u32[]{:S(2)}) collective-permute-start(f32[2,256]{0,1:T(8,128)S(1)} %slice.48), channel_id=1, source_target_pairs={{0,4},{4,8},{8,12},{12,16},{16,20},{20,24},{24,28},{28,32},{32,36}... | collective-permute-start | bytes 6152 | tf_op jit(solution)/shard_map/ppermute | solution.py:20
  7.0 0.1 slice.35
  7.1 1.9 %collective-permute-start = (s32[2]{0:T(128)S(1)}, s32[2]{0:T(128)S(1)}, u32[]{:S(2)}, u32[]{:S(2)}) collective-permute-start(s32[2]{0:T(128)S(1)} %slice.35), channel_id=1, source_target_pairs={{0,4},{4,8},{8,12},{12,16},{16,20},{20,24},{24,28},{28,32},{32,36}... | collective-permute-start | bytes 32 | tf_op jit(solution)/shard_map/ppermute | solution.py:20
  9.0 0.0 copy-done.6
  9.0 0.1 copy.20
  9.2 0.1 eq.37
  9.3 0.1 eq.33
  9.5 0.0 copy-start.1
  9.5 0.1 copy.15
  9.6 0.1 copy.22
  9.8 0.2 fusion.26
  10.0 0.1 add_add_fusion
  10.1 0.1 copy.19
  10.2 0.1 mul.103
  10.3 0.2 fusion.27
  10.5 0.0 collective-permute-done
  10.5 0.1 pad_add_fusion
  10.6 0.1 slice_compare_fusion.1
  10.7 0.0 collective-permute-done.1
  10.7 0.5 fusion.23
  11.3 0.7 pad_maximum_fusion.1
  12.0 4.0 %all-to-all-start = ((bf16[4,128,256]{1,2,0:T(8,128)(2,1)}), bf16[4,128,256]{1,2,0:T(8,128)(2,1)S(1)}, u32[]{:S(2)}, u32[]{:S(2)}) async-start(bf16[4,128,256]{1,2,0:T(8,128)(2,1)} %pad_maximum_fusion.1), calls=%async_computation | async-start | bytes 524288 | tf_op jit(solution)/shard_map/all_to_all | solution.py:7
  16.0 5.7 %all-to-all-done = bf16[4,128,256]{1,2,0:T(8,128)(2,1)S(1)} async-done(((bf16[4,128,256]{1,2,0:T(8,128)(2,1)}), bf16[4,128,256]{1,2,0:T(8,128)(2,1)S(1)}, u32[]{:S(2)}, u32[]{:S(2)}) %all-to-all-start) | async-done | bytes 262176 | tf_op jit(solution)/shard_map/all_to_all | solution.py:7
  21.7 0.0 copy-done.1
  21.7 3.0 %multiply_reduce_fusion.1 = (f32[128]{0:T(128)S(1)}, f32[128,2048]{1,0:T(8,128)S(1)}) fusion(bf16[128,1024]{0,1:T(8,128)(2,1)S(1)} %bitcast.43, bf16[1024,2048]{1,0:T(8,128)(2,1)} %param.19, bf16[128,2048]{1,0:T(8,128)(2,1)S(1)} %copy-done.1), kind=kOutput, calls=%fused_computation.16 | convolution fusion | flops 538443648 | bytes 6029824 | tf_op jit(solution)/shard_map/dot_general | solution.py:59
  24.8 0.2 multiply_convert_fusion.1
  24.9 0.6 broadcast_in_dim.36
  25.6 1.2 reshape.105
  26.8 3.5 %scatter_custom_fusion = bf16[512,2048]{1,0:T(8,128)(2,1)S(1)} fusion(s32[256]{0:T(256)S(1)} %bitcast.48, bf16[256,2048]{1,0:T(8,128)(2,1)} %reshape.105, bf16[]{:T(256)} %constant.6.clone.1), kind=kCustom, calls=%fused_computation.17 | custom fusion | bytes 2097664 | tf_op jit(solution)/shard_map/scatter | solution.py:78
  30.3 2.2 %reshape.88 = bf16[128,4,2048]{2,1,0:T(4,128)(2,1)} reshape(bf16[512,2048]{1,0:T(8,128)(2,1)S(1)} %scatter_custom_fusion) | data formatting | bytes 4194304 | tf_op jit(solution)/shard_map/reshape | solution.py:84
  32.5 40.5 %all_to_all.15 = bf16[128,4,2048]{2,1,0:T(4,128)(2,1)S(1)} all-to-all(bf16[128,4,2048]{2,1,0:T(4,128)(2,1)} %reshape.88), channel_id=1, replica_groups=mesh['sp'=32,'tp'=4] {'sp','tp'}, dimensions={0} | all-to-all | bytes 4194304 | tf_op jit(solution)/shard_map/all_to_all | solution.py:83
  73.0 2.0 %reshape.89 = bf16[512,2048]{1,0:T(8,128)(2,1)} reshape(bf16[128,4,2048]{2,1,0:T(4,128)(2,1)S(1)} %all_to_all.15) | data formatting | bytes 4194304 | tf_op jit(solution)/shard_map/reshape | solution.py:91
  75.1 6.6 %fusion.4 = f32[512,1024]{1,0:T(8,128)} fusion(bf16[512,2048]{1,0:T(8,128)(2,1)} %reshape.89, bf16[1,2048,1024]{2,1,0:T(8,128)(2,1)} %param.23), kind=kOutput, calls=%fused_computation.6 | convolution fusion | flops 2147483648 | bytes 8388608 | tf_op jit(solution)/shard_map/dot_general | solution.py:24
  81.7 9.9 %fusion.6 = bf16[512,2048]{1,0:T(8,128)(2,1)} fusion(bf16[1,1024,2048]{2,1,0:T(8,128)(2,1)} %param.25, f32[512,1024]{1,0:T(8,128)} %fusion.4, bf16[512,2048]{1,0:T(8,128)(2,1)S(1)} %copy-done, bf16[1,2048,1024]{2,1,0:T(8,128)(2,1)} %param.24), kind=kOutput, calls=%fused_computation.8 | convolution fusion | flops 4299161600 | bytes 14680064 | tf_op jit(solution)/shard_map/dot_general | solution.py:27
  91.6 4.1 %reshape.90 = bf16[128,4,2048]{2,1,0:T(4,128)(2,1)} reshape(bf16[512,2048]{1,0:T(8,128)(2,1)} %fusion.6) | data formatting | bytes 4194304 | tf_op jit(solution)/shard_map/reshape | solution.py:93
  95.7 5.0 %all-to-all-start.2 = ((bf16[128,4,2048]{2,1,0:T(4,128)(2,1)}), bf16[128,4,2048]{2,1,0:T(4,128)(2,1)}, u32[]{:S(2)}, u32[]{:S(2)}) async-start(bf16[128,4,2048]{2,1,0:T(4,128)(2,1)} %reshape.90), calls=%async_computation.2 | async-start | bytes 4194304 | tf_op jit(solution)/shard_map/all_to_all | solution.py:94
  100.7 0.1 copy.18
  100.8 30.4 %all-to-all-done.2 = bf16[128,4,2048]{2,1,0:T(4,128)(2,1)} async-done(((bf16[128,4,2048]{2,1,0:T(4,128)(2,1)}), bf16[128,4,2048]{2,1,0:T(4,128)(2,1)}, u32[]{:S(2)}, u32[]{:S(2)}) %all-to-all-start.2) | async-done | bytes 2097184 | tf_op jit(solution)/shard_map/all_to_all | solution.py:94
  131.2 2.5 %reshape.91 = bf16[512,2048]{1,0:T(8,128)(2,1)S(1)} reshape(bf16[128,4,2048]{2,1,0:T(4,128)(2,1)} %all-to-all-done.2) | data formatting | bytes 4194304 | tf_op jit(solution)/shard_map/reshape | solution.py:96
  133.8 2.3 %gather_fusion = bf16[256,2048]{1,0:T(8,128)(2,1)} fusion(bf16[512,2048]{1,0:T(8,128)(2,1)S(1)} %reshape.91, s32[1024]{0:T(1024)S(1)} %pad_clamp_fusion), kind=kCustom, calls=%fused_computation | custom fusion | bytes 2098176 | tf_op jit(solution)/shard_map/gather | solution.py:96
  136.1 2.4 %reshape.92 = f32[128,2,2048]{2,1,0:T(2,128)S(1)} reshape(bf16[256,2048]{1,0:T(8,128)(2,1)} %gather_fusion) | data formatting | bytes 3145728 | tf_op jit(solution)/shard_map/convert_element_type | solution.py:98
  138.5 3.2 %multiply_reduce_fusion = f32[128,2048]{1,0:T(8,128)S(1)} fusion(f32[128,2,2048]{2,1,0:T(2,128)S(1)} %reshape.92, f32[128,2]{1,0:T(8,128)S(1)} %copy.18), kind=kLoop, calls=%fused_computation.12 | loop fusion | flops 786432 | bytes 3146752 | tf_op jit(solution)/shard_map/reduce_sum | solution.py:100
  141.7 0.9 add_convert_fusion
  (22 shorter events, 0.2 us)
Async XLA Ops:
  0.0 7.0 %copy-start.4 = (s32[512]{0:T(512)S(1)}, s32[512]{0:T(512)}, u32[]{:S(2)}) copy-start(s32[512]{0:T(512)} %param.17) | copy-start | bytes 6148
  0.0 9.0 %copy-start.6 = (s32[128,2]{0,1:T(2,128)S(1)}, s32[128,2]{0,1:T(2,128)}, u32[]{:S(2)}) copy-start(s32[128,2]{0,1:T(2,128)} %param.21) | copy-start | bytes 3076
  0.0 9.4 %copy-start.5 = (bf16[3,256]{1,0:T(4,128)(2,1)S(1)}, bf16[3,256]{1,0:T(4,128)(2,1)}, u32[]{:S(2)}) copy-start(bf16[3,256]{1,0:T(4,128)(2,1)} %param.16) | copy-start | bytes 4612
  0.0 9.5 %copy-start.2 = (bf16[512,256]{1,0:T(8,128)(2,1)S(1)}, bf16[512,256]{1,0:T(8,128)(2,1)}, u32[]{:S(2)}) copy-start(bf16[512,256]{1,0:T(8,128)(2,1)} %param.15) | copy-start | bytes 786436
  2.4 8.3 %collective-permute-start.1 = (f32[2,256]{0,1:T(8,128)S(1)}, f32[2,256]{0,1:T(8,128)S(1)}, u32[]{:S(2)}, u32[]{:S(2)}) collective-permute-start(f32[2,256]{0,1:T(8,128)S(1)} %slice.48), channel_id=1, source_target_pairs={{0,4},{4,8},{8,12},{12,16},{16,20},{20,24},{24,28},{28,32},{32,36}... | collective-permute-start | bytes 6152 | tf_op jit(solution)/shard_map/ppermute | solution.py:20
  7.1 3.4 %collective-permute-start = (s32[2]{0:T(128)S(1)}, s32[2]{0:T(128)S(1)}, u32[]{:S(2)}, u32[]{:S(2)}) collective-permute-start(s32[2]{0:T(128)S(1)} %slice.35), channel_id=1, source_target_pairs={{0,4},{4,8},{8,12},{12,16},{16,20},{20,24},{24,28},{28,32},{32,36}... | collective-permute-start | bytes 32 | tf_op jit(solution)/shard_map/ppermute | solution.py:20
  9.5 12.2 %copy-start.1 = (bf16[128,2048]{1,0:T(8,128)(2,1)S(1)}, bf16[128,2048]{1,0:T(8,128)(2,1)}, u32[]{:S(2)}) copy-start(bf16[128,2048]{1,0:T(8,128)(2,1)} %param.18) | copy-start | bytes 1572868
  12.0 9.7 %all-to-all-start = ((bf16[4,128,256]{1,2,0:T(8,128)(2,1)}), bf16[4,128,256]{1,2,0:T(8,128)(2,1)S(1)}, u32[]{:S(2)}, u32[]{:S(2)}) async-start(bf16[4,128,256]{1,2,0:T(8,128)(2,1)} %pad_maximum_fusion.1), calls=%async_computation | async-start | bytes 524288 | tf_op jit(solution)/shard_map/all_to_all | solution.py:7
  21.7 3.0 %copy-start.3 = (f32[2048]{0:T(1024)S(1)}, f32[2048]{0:T(1024)}, u32[]{:S(2)}) copy-start(f32[2048]{0:T(1024)} %param.20) | copy-start | bytes 24580
  75.1 6.6 %copy-start = (bf16[512,2048]{1,0:T(8,128)(2,1)S(1)}, bf16[512,2048]{1,0:T(8,128)(2,1)}, u32[]{:S(2)}) copy-start(bf16[512,2048]{1,0:T(8,128)(2,1)} %reshape.89) | copy-start | bytes 6291460
  95.7 5.0 %copy-start.7 = (f32[128,2]{0,1:T(2,128)S(1)}, f32[128,2]{0,1:T(2,128)}, u32[]{:S(2)}) copy-start(f32[128,2]{0,1:T(2,128)} %param.22) | copy-start | bytes 3076
  95.7 35.5 %all-to-all-start.2 = ((bf16[128,4,2048]{2,1,0:T(4,128)(2,1)}), bf16[128,4,2048]{2,1,0:T(4,128)(2,1)}, u32[]{:S(2)}, u32[]{:S(2)}) async-start(bf16[128,4,2048]{2,1,0:T(4,128)(2,1)} %reshape.90), calls=%async_computation.2 | async-start | bytes 4194304 | tf_op jit(solution)/shard_map/all_to_all | solution.py:94
